TPU v7x, 32 devices: a whole 2x2x4 slice. The times are simulated.
32 devices in a mesh: dp: 4 (over y, x), kv: 4 (over z), tp: 2 (over core).
Axes of the slice: x: 2, y: 2, z: 4, core: 2. Of those that a mesh axis runs over, the one named last changes fastest.
Arguments:
- tokens: bfloat16 [32, 4096], P('dp', ('kv', 'tp')), as said below
- query_weight: bfloat16 [4096, 16, 128], P(None, 'tp', 'kv'), may hold values from -0.09375 to 0.09375
- key_weight: bfloat16 [4096, 16, 128], P(None, 'tp', 'kv'), may hold values from -0.09375 to 0.09375
- value_weight: bfloat16 [4096, 16, 256], P(None, 'tp', 'kv'), may hold values from -0.09375 to 0.09375
- gate_weight: bfloat16 [4096, 16, 256], P(None, 'tp', 'kv'), may hold values from -0.09375 to 0.09375
- decay_weight: bfloat16 [4096, 16, 128], P(None, 'tp', 'kv'), may hold values from -0.09375 to 0.09375
- decay_bias: float32 [16, 128], P('tp'), may hold values from -8 to 2
- states: float32 [32, 16, 128, 256], P(('dp', 'kv'), 'tp'), may hold values from -4 to 4
- head_gain: float32 [16, 256], P('tp'), may hold values from 0.1 to 1.9
- out_weight: bfloat16 [4096, 4096], P(None, ('kv', 'tp')), as said below
- norm1_gain: float32 [4096], P(('kv', 'tp')), may hold values from 0.1 to 1.9
- norm1_bias: float32 [4096], P(('kv', 'tp')), may hold values from -3 to 3
- up_weight: bfloat16 [4096, 16384], P(None, ('kv', 'tp')), may hold values from -0.09375 to 0.09375
- down_weight: bfloat16 [16384, 4096], P(('kv', 'tp')), as said below
- norm2_gain: float32 [4096], P(('kv', 'tp')), may hold values from 0.1 to 1.9
- norm2_bias: float32 [4096], P(('kv', 'tp')), may hold values from -3 to 3
Outputs:
- layer_out: bfloat16 [32, 4096], P('dp', ('kv', 'tp'))
- new_states: float32 [32, 16, 128, 256], P(('dp', 'kv'), 'tp')
Inputs may be any that keep to these rules, and one draw needn't show every extreme that they name: `tokens`: each block of 64 features has its own scale. `out_weight`: entries lie within 13 / sqrt(4096) of zero. `down_weight`: entries lie within 14 / sqrt(16384) of zero.
All inputs are finite; a program needn't handle non-finite values.
Results may differ from a plain program's by a relative error of at most 0.009.
Values may be sent and summed in bfloat16 or wider, within the bound.
A program may use at most 128 MiB of HBM per device.

v0:
```python
import jax
import jax.numpy as jnp
from jax import lax
from jax.sharding import PartitionSpec as P

D = 4096
KEY_DIM = 128
ALPHA = 2.0**0.5
TAU = 16.0
LN_EPS = 1e-05
RMS_EPS = 1e-06


def project_flat(inputs, weight):
    flattened = weight.reshape(weight.shape[0], -1)
    return jnp.dot(inputs, flattened, preferred_element_type=jnp.float32).astype(jnp.bfloat16)


def normalize(inputs, average, spread, row_gain, row_shift):
    return ((inputs - average) * lax.rsqrt(spread + LN_EPS) * row_gain + row_shift).astype(
        jnp.bfloat16
    )


def body(
    tokens,
    query_weight,
    key_weight,
    value_weight,
    gate_weight,
    decay_weight,
    decay_bias,
    states,
    head_gain,
    out_weight,
    norm1_gain,
    norm1_bias,
    up_weight,
    down_weight,
    norm2_gain,
    norm2_bias,
):
    whole = lax.all_gather(tokens, ("kv", "tp"), axis=1, tiled=True)
    weights_list = (query_weight, key_weight, decay_weight, value_weight, gate_weight)
    packed = jnp.concatenate([project_flat(whole, weight) for weight in weights_list], axis=1)
    arrived = lax.all_to_all(packed, "kv", split_axis=0, concat_axis=0, tiled=True)
    groups = lax.axis_size("kv")
    seq_count = whole.shape[0] // groups
    local_heads = query_weight.shape[1]
    unpacked = []
    start = 0
    for weight in weights_list:
        channels = weight.shape[2]
        width = local_heads * channels
        block = arrived[:, start : start + width].reshape(groups, seq_count, local_heads, channels)
        block = block.transpose(1, 2, 0, 3).reshape(seq_count, local_heads, groups * channels)
        unpacked.append(block.astype(jnp.float32))
        start = start + width
    query_rows = unpacked[0] * KEY_DIM ** (-0.5)
    key_rows = unpacked[1]
    decay_rows = unpacked[2]
    value_rows = unpacked[3]
    gate_rows = unpacked[4]
    retain = jnp.exp(jax.nn.log_sigmoid(decay_rows + decay_bias) / TAU)
    new_states = retain[..., None] * states + key_rows[..., :, None] * value_rows[..., None, :]
    readout = jnp.einsum("shk,shkv->shv", query_rows, new_states, precision=lax.Precision.HIGHEST)
    readout = (
        readout
        * lax.rsqrt(jnp.mean(readout * readout, axis=-1, keepdims=True) + RMS_EPS)
        * head_gain
    )
    attended = (readout * jax.nn.silu(gate_rows)).astype(jnp.bfloat16)
    seq_count, local_heads, value_width = attended.shape
    flat_width = local_heads * value_width
    collected = lax.all_gather(
        attended.reshape(1, seq_count, flat_width), ("kv", "tp"), axis=0, tiled=True
    )
    halves = lax.axis_size("tp")
    collected = collected.reshape(-1, halves, seq_count, flat_width)
    columns = out_weight.shape[1]
    out_parts = out_weight.reshape(halves, flat_width, columns)
    mixed_heads = jnp.einsum(
        "atsc,tcd->asd", collected, out_parts, preferred_element_type=jnp.float32
    ).reshape(-1, columns)
    residual_one = ALPHA * tokens.astype(jnp.float32) + mixed_heads
    offset = lax.axis_index(("kv", "tp")) * columns
    totals = lax.psum(
        (
            jnp.sum(residual_one, axis=-1, keepdims=True),
            jnp.sum(residual_one * residual_one, axis=-1, keepdims=True),
        ),
        ("kv", "tp"),
    )
    average = totals[0] / D
    spread = totals[1] / D - average * average
    normed_own = normalize(residual_one, average, spread, norm1_gain, norm1_bias)
    normed = lax.all_gather(normed_own, ("kv", "tp"), axis=1, tiled=True)
    lifted = jnp.dot(normed, up_weight, preferred_element_type=jnp.float32)
    hidden = jnp.square(jax.nn.relu(lifted)).astype(jnp.bfloat16)
    mixer_term = jnp.dot(hidden, down_weight, preferred_element_type=jnp.float32)
    mixer_all = lax.psum(mixer_term, ("kv", "tp"))
    residual_two = ALPHA * normed.astype(jnp.float32) + mixer_all
    average = jnp.sum(residual_two, axis=-1, keepdims=True) / D
    spread = jnp.sum(residual_two * residual_two, axis=-1, keepdims=True) / D - average * average
    own_rows = lax.dynamic_slice_in_dim(residual_two, offset, columns, 1)
    layer_out = normalize(own_rows, average, spread, norm2_gain, norm2_bias)
    return (layer_out, new_states)


def solution(mesh):
    placed = (
        P("dp", ("kv", "tp")),
        P(None, "tp", "kv"),
        P(None, "tp", "kv"),
        P(None, "tp", "kv"),
        P(None, "tp", "kv"),
        P(None, "tp", "kv"),
        P("tp", None),
        P(("dp", "kv"), "tp", None, None),
        P("tp", None),
        P(None, ("kv", "tp")),
        P(("kv", "tp")),
        P(("kv", "tp")),
        P(None, ("kv", "tp")),
        P(("kv", "tp"), None),
        P(("kv", "tp")),
        P(("kv", "tp")),
    )
    return jax.shard_map(
        body,
        mesh=mesh,
        in_specs=placed,
        out_specs=(P("dp", ("kv", "tp")), P(("dp", "kv"), "tp", None, None)),
        check_vma=False,
    )
```

profile of v0, /device:TPU:0, one launch (start us, length us, event | category | flops | bytes accessed | tf_op | source)
XLA Modules:
  0.0 167.2 jit_solution(12161936013294554536)
XLA Ops:
  7.2 0.0 copy-start
  7.2 0.0 all-reduce.3.cloned.1.call-start
  7.2 0.0 copy-start.4
  7.2 16.0 %all_gather.9 = bf16[8,4096]{1,0:T(8,128)(2,1)S(1)} all-gather(bf16[8,512]{1,0:T(8,128)(2,1)} %param.16), channel_id=1, replica_groups=mesh['dp'=4,'kv'=4,'tp'=2] {'kv','tp'}, dimensions={1}, use_global_device_ids=true | all-gather | bytes 73728 | tf_op jit(solution)/shard_map/all_gather | solution.py:43
  23.3 0.0 copy-done
  23.3 0.6 fusion.7
  23.9 0.0 copy-done.4
  23.9 0.7 fusion.6
  24.6 2.6 %fusion.5 = bf16[8,1792]{1,0:T(8,128)(2,1)S(1)} fusion(bf16[8,1792]{1,0:T(8,128)(2,1)S(1)} %fusion.6, bf16[8,4096]{1,0:T(8,128)(2,1)S(1)} %all_gather.9, bf16[4096,256]{0,1:T(8,128)(2,1)} %bitcast.60), kind=kOutput, calls=%fused_computation.11 | convolution fusion | flops 16779264 | bytes 2166784 | tf_op jit(solution)/shard_map/dot_general | solution.py:16
  27.2 0.0 copy-done.2
  27.2 1.2 fusion.4
  28.4 1.0 copy-done.3
  29.4 1.2 fusion.3
  30.6 10.1 %all_to_all.12 = bf16[4,2,1792]{2,1,0:T(2,128)(2,1)S(1)} all-to-all(bf16[4,2,1792]{2,1,0:T(2,128)(2,1)S(1)} %all_to_all.8), channel_id=1, replica_groups=mesh['dp'=4,'kv'=4,'tp'=2] {'kv'}, dimensions={0} | all-to-all | bytes 57344 | tf_op jit(solution)/shard_map/all_to_all | solution.py:46
  40.7 0.1 reshape.138
  40.8 0.1 reshape.134
  40.9 0.1 reshape.136
  41.0 0.1 reshape.132
  41.1 0.1 reshape.137
  41.2 0.1 reshape.133
  41.3 0.1 mul.135
  41.4 0.1 reshape.140
  41.4 0.0 copy-done.7
  41.5 1.9 %multiply_add_fusion = f32[2,8,128,256]{3,2,1,0:T(8,128)S(1)} fusion(f32[2,8,128,256]{3,2,1,0:T(8,128)} %param.23, f32[2,8,256]{2,1,0:T(8,128)S(1)} %reshape.134, f32[2,8,128]{2,1,0:T(8,128)S(1)} %reshape.133, f32[2,8,128]{2,1,0:T(8,128)S(1)} %fusion.16), kind=kLoop, calls=%fused_computation.3 | loop fusion | flops 1572864 | bytes 4227072 | tf_op jit(solution)/shard_map/add | solution.py:65
  43.4 0.0 copy-start.1
  43.4 0.0 copy-start.6
  43.4 0.0 copy-start.5
  43.4 1.3 copy-done.1
  44.7 1.1 fusion.20
  45.8 0.1 fusion.10
  45.9 0.1 reshape.139
  46.0 0.1 reshape.135
  46.1 0.0 copy-done.6
  46.1 0.1 fusion.13
  46.2 14.0 %all_gather.10 = bf16[8,2,2048]{2,1,0:T(2,128)(2,1)S(1)} all-gather(bf16[1,2,2048]{2,1,0:T(2,128)(2,1)S(1)} %reshape.129), channel_id=1, replica_groups=mesh['dp'=4,'kv'=4,'tp'=2] {'kv','tp'}, dimensions={0}, use_global_device_ids=true | all-gather | bytes 73728 | tf_op jit(solution)/shard_map/all_gather | solution.py:75
  60.3 0.0 copy-done.5
  60.3 0.0 copy-start.8
  60.3 0.0 copy-start.9
  60.3 3.0 %fusion.19 = (f32[8]{0:T(128)S(1)}, f32[8]{0:T(128)S(1)}, f32[8,512]{1,0:T(8,128)S(1)}) fusion(bf16[8,2048,2]{1,0,2:T(8,128)(2,1)S(1)} %dot_general.38, bf16[2,2048,512]{2,1,0:T(8,128)(2,1)} %bitcast.56, bf16[8,512]{1,0:T(8,128)(2,1)S(1)} %copy-done.5), kind=kOutput, calls=%fused_computation.45 | convolution fusion | flops 33578992 | bytes 4284480 | tf_op jit(solution)/shard_map/atsc,tcd->asd/dot_general | solution.py:82
  63.3 14.2 %all-reduce = (f32[8,1]{0,1:T(1,128)S(1)}, f32[8,1]{0,1:T(1,128)S(1)}) all-reduce(f32[8,1]{0,1:T(1,128)S(1)} %bitcast.69, f32[8,1]{0,1:T(1,128)S(1)} %bitcast.68), channel_id=1, replica_groups=mesh['dp'=4,'kv'=4,'tp'=2] {'kv','tp'}, use_global_device_ids=true, to_apply=%region_4.5 | all-reduce | flops 16 | bytes 128 | tf_op jit(solution)/shard_map/psum | solution.py:87
  77.6 0.0 copy-done.9
  77.6 0.1 add_convert_fusion.1
  77.7 14.0 %all_gather.11 = bf16[8,4096]{1,0:T(8,128)(2,1)S(1)} all-gather(bf16[8,512]{1,0:T(8,128)(2,1)S(1)} %add_convert_fusion.1), channel_id=1, replica_groups=mesh['dp'=4,'kv'=4,'tp'=2] {'kv','tp'}, dimensions={1}, use_global_device_ids=true | all-gather | bytes 73728 | tf_op jit(solution)/shard_map/all_gather | solution.py:97
  91.6 13.5 %fusion.8 = f32[8,4096]{1,0:T(8,128)} fusion(bf16[2048,4096]{1,0:T(8,128)(2,1)} %param.29, bf16[8,4096]{1,0:T(8,128)(2,1)S(1)} %all_gather.11, bf16[4096,2048]{1,0:T(8,128)(2,1)} %param.28), kind=kOutput, calls=%fused_computation.16 | convolution fusion | flops 268484608 | bytes 33751040 | tf_op jit(solution)/shard_map/dot_general | solution.py:100
  105.2 0.0 all-reduce.3.cloned.1.call-update
  105.2 53.4 %all-reduce.3.cloned.1.call-done = f32[8,4096]{1,0:T(8,128)} async-done(((f32[8,4096]{1,0:T(8,128)}), f32[8,4096]{1,0:T(8,128)}) %all-reduce.3.cloned.1.call-update) | async-done | bytes 131088 | tf_op jit(solution)/shard_map/psum | solution.py:101
  158.5 1.1 fusion.18
  159.6 0.7 add_convert_fusion
  (25 shorter events, 0.3 us)
Async XLA Ops:
  7.2 16.1 %copy-start = (bf16[4096,8,32]{0,2,1:T(8,128)(2,1)S(1)}, bf16[4096,8,32]{0,2,1:T(8,128)(2,1)}, u32[]{:S(2)}) copy-start(bf16[4096,8,32]{0,2,1:T(8,128)(2,1)} %param.17) | copy-start | bytes 6291460
  7.2 151.4 %all-reduce.3.cloned.1.call-start = ((), (), s32[]{:S(2)}) async-start(), calls=%async_computation.1 | async-start | bytes 262144 | tf_op jit(solution)/shard_map/psum | solution.py:101
  7.2 16.7 %copy-start.4 = (bf16[4096,8,32]{0,2,1:T(8,128)(2,1)S(1)}, bf16[4096,8,32]{0,2,1:T(8,128)(2,1)}, u32[]{:S(2)}) copy-start(bf16[4096,8,32]{0,2,1:T(8,128)(2,1)} %param.18) | copy-start | bytes 6291460
  23.9 3.2 %copy-start.2 = (bf16[4096,8,64]{0,2,1:T(8,128)(2,1)S(1)}, bf16[4096,8,64]{0,2,1:T(8,128)(2,1)}, u32[]{:S(2)}) copy-start(bf16[4096,8,64]{0,2,1:T(8,128)(2,1)} %param.19) | copy-start | bytes 12582916
  27.2 2.2 %copy-start.3 = (bf16[4096,8,64]{0,2,1:T(8,128)(2,1)S(1)}, bf16[4096,8,64]{0,2,1:T(8,128)(2,1)}, u32[]{:S(2)}) copy-start(bf16[4096,8,64]{0,2,1:T(8,128)(2,1)} %param.20) | copy-start | bytes 12582916
  29.4 12.1 %copy-start.7 = (f32[8,128]{1,0:T(8,128)S(1)}, f32[8,128]{1,0:T(8,128)}, u32[]{:S(2)}) copy-start(f32[8,128]{1,0:T(8,128)} %param.22) | copy-start | bytes 12292
  43.4 1.3 copy-start.1
  43.4 2.7 %copy-start.6 = (f32[8,256]{1,0:T(8,128)S(1)}, f32[8,256]{1,0:T(8,128)}, u32[]{:S(2)}) copy-start(f32[8,256]{1,0:T(8,128)} %param.24) | copy-start | bytes 24580
  43.4 16.9 %copy-start.5 = (bf16[8,512]{1,0:T(8,128)(2,1)S(1)}, bf16[8,512]{1,0:T(8,128)(2,1)}, u32[]{:S(2)}) copy-start(bf16[8,512]{1,0:T(8,128)(2,1)} %param.16) | copy-start | bytes 24580
  60.3 17.3 %copy-start.8 = (f32[512]{0:T(512)S(1)}, f32[512]{0:T(512)}, u32[]{:S(2)}) copy-start(f32[512]{0:T(512)} %param.27) | copy-start | bytes 6148
  60.3 17.3 %copy-start.9 = (f32[512]{0:T(512)S(1)}, f32[512]{0:T(512)}, u32[]{:S(2)}) copy-start(f32[512]{0:T(512)} %param.26) | copy-start | bytes 6148
  91.6 68.0 %copy-start.10 = (f32[512]{0:T(512)S(1)}, f32[512]{0:T(512)}, u32[]{:S(2)}) copy-start(f32[512]{0:T(512)} %param.31) | copy-start | bytes 6148
  91.6 68.0 %copy-start.11 = (f32[512]{0:T(512)S(1)}, f32[512]{0:T(512)}, u32[]{:S(2)}) copy-start(f32[512]{0:T(512)} %param.30) | copy-start | bytes 6148
Sparse Core Ops, SparseCore 0:
  105.3 53.1 all-reduce.2
where the time goes:
time: 167 us
  blocking collectives  68.3 us (41%)
  waiting for transfers between devices  53.4 us (32%)
  matrix products  23.9 us (14%)
  between operations  14.2 us (9%)
  other arithmetic  4 us (2%)
  local copies, waits for them, and re-layouts  3.36 us (2%)
    psum x1, waiting for transfers between devices, body(): mixer_all = lax.psum(mixer_term, ('kv', 'tp'))  53.4 us
    all_gather x1, blocking collectives, body(): whole = lax.all_gather(tokens, ('kv', 'tp'), axis=1, tiled=True)  16 us
    psum x1, blocking collectives, body(): lax.psum((jnp.sum(residual_one, axis=-1, keepdims=True), jnp.sum(residual...  14.2 us
    all_gather x1, blocking collectives, body(): lax.all_gather(attended.reshape(1, seq_count, flat_width), ('kv', 'tp'),...  14 us
    all_gather x1, blocking collectives, body(): normed = lax.all_gather(normed_own, ('kv', 'tp'), axis=1, tiled=True)  14 us
    dot_general x1, matrix products, body(): jnp.dot(hidden, down_weight, preferred_element_type=jnp.float32)  13.5 us
    all_to_all x1, blocking collectives, body(): lax.all_to_all(packed, 'kv', split_axis=0, concat_axis=0, tiled=True)  10.1 us
    dot_general x5, matrix products, project_flat(): jnp.dot(inputs, flattened, preferred_element_type=jnp.float32)  6.25 us
  transfers between devices with their start and end apart: 1, of which 1 were waited for; matrix products, arithmetic and copies ran while one was open for 0% of the time, Pallas kernels for 0%

commit v1 on v0

--- a/solution.py
+++ b/solution.py
@@ -9,6 +9,7 @@
 TAU = 16.0
 LN_EPS = 1e-05
 RMS_EPS = 1e-06
+_solve_panel = lambda x_local: jax.lax.psum(jax.lax.psum(x_local, "tp"), "kv")
 
 
 def project_flat(inputs, weight):
@@ -84,12 +85,11 @@
     ).reshape(-1, columns)
     residual_one = ALPHA * tokens.astype(jnp.float32) + mixed_heads
     offset = lax.axis_index(("kv", "tp")) * columns
-    totals = lax.psum(
+    totals = _solve_panel(
         (
             jnp.sum(residual_one, axis=-1, keepdims=True),
             jnp.sum(residual_one * residual_one, axis=-1, keepdims=True),
-        ),
-        ("kv", "tp"),
+        )
     )
     average = totals[0] / D
     spread = totals[1] / D - average * average

time: 167 us -> 165 us (0.988)
  blocking collectives: 68.3 us -> 65.6 us
    psum x1 -> x2, blocking collectives: 14.2 us -> 11.5 us  [the longest x1 9.04 us: jax.lax.psum(jax.lax.psum(x_local, 'tp'), 'kv')]
where the time goes in v1:
time: 165 us
  blocking collectives  65.6 us (40%)
  waiting for transfers between devices  54.1 us (33%)
  matrix products  23.9 us (14%)
  between operations  14.2 us (9%)
  other arithmetic  4 us (2%)
  local copies, waits for them, and re-layouts  3.36 us (2%)
    psum x1, waiting for transfers between devices, body(): mixer_all = lax.psum(mixer_term, ('kv', 'tp'))  54.1 us
    all_gather x1, blocking collectives, body(): whole = lax.all_gather(tokens, ('kv', 'tp'), axis=1, tiled=True)  16 us
    all_gather x1, blocking collectives, body(): lax.all_gather(attended.reshape(1, seq_count, flat_width), ('kv', 'tp'),...  14 us
    all_gather x1, blocking collectives, body(): normed = lax.all_gather(normed_own, ('kv', 'tp'), axis=1, tiled=True)  14 us
    dot_general x1, matrix products, body(): jnp.dot(hidden, down_weight, preferred_element_type=jnp.float32)  13.5 us
    all_to_all x1, blocking collectives, body(): lax.all_to_all(packed, 'kv', split_axis=0, concat_axis=0, tiled=True)  10.1 us
    psum x1, blocking collectives, jax.lax.psum(jax.lax.psum(x_local, 'tp'), 'kv')  9.04 us
    dot_general x5, matrix products, project_flat(): jnp.dot(inputs, flattened, preferred_element_type=jnp.float32)  6.25 us
  transfers between devices with their start and end apart: 1, of which 1 were waited for; matrix products, arithmetic and copies ran while one was open for 0% of the time, Pallas kernels for 0%

profile of v1, /device:TPU:0, one launch (start us, length us, event | category | flops | bytes accessed | tf_op | source)
XLA Modules:
  0.0 165.2 jit_solution(6887284719110287231)
XLA Ops:
  7.2 0.0 copy-start
  7.2 0.0 all-reduce.4.cloned.1.call-start
  7.2 0.0 copy-start.4
  7.2 16.0 %all_gather.9 = bf16[8,4096]{1,0:T(8,128)(2,1)S(1)} all-gather(bf16[8,512]{1,0:T(8,128)(2,1)} %param.16), channel_id=1, replica_groups=mesh['dp'=4,'kv'=4,'tp'=2] {'kv','tp'}, dimensions={1}, use_global_device_ids=true | all-gather | bytes 73728 | tf_op jit(solution)/shard_map/all_gather | solution.py:44
  23.3 0.0 copy-done
  23.3 0.6 fusion.7
  23.9 0.0 copy-done.4
  23.9 0.7 fusion.6
  24.6 2.6 %fusion.5 = bf16[8,1792]{1,0:T(8,128)(2,1)S(1)} fusion(bf16[8,1792]{1,0:T(8,128)(2,1)S(1)} %fusion.6, bf16[8,4096]{1,0:T(8,128)(2,1)S(1)} %all_gather.9, bf16[4096,256]{0,1:T(8,128)(2,1)} %bitcast.60), kind=kOutput, calls=%fused_computation.11 | convolution fusion | flops 16779264 | bytes 2166784 | tf_op jit(solution)/shard_map/dot_general | solution.py:17
  27.2 0.0 copy-done.2
  27.2 1.2 fusion.4
  28.4 1.0 copy-done.3
  29.4 1.2 fusion.3
  30.6 10.1 %all_to_all.12 = bf16[4,2,1792]{2,1,0:T(2,128)(2,1)S(1)} all-to-all(bf16[4,2,1792]{2,1,0:T(2,128)(2,1)S(1)} %all_to_all.8), channel_id=1, replica_groups=mesh['dp'=4,'kv'=4,'tp'=2] {'kv'}, dimensions={0} | all-to-all | bytes 57344 | tf_op jit(solution)/shard_map/all_to_all | solution.py:47
  40.7 0.1 reshape.138
  40.8 0.1 reshape.134
  40.9 0.1 reshape.136
  41.0 0.1 reshape.132
  41.1 0.1 reshape.137
  41.2 0.1 reshape.133
  41.3 0.1 mul.135
  41.4 0.1 reshape.140
  41.4 0.0 copy-done.7
  41.5 1.9 %multiply_add_fusion = f32[2,8,128,256]{3,2,1,0:T(8,128)S(1)} fusion(f32[2,8,128,256]{3,2,1,0:T(8,128)} %param.23, f32[2,8,256]{2,1,0:T(8,128)S(1)} %reshape.134, f32[2,8,128]{2,1,0:T(8,128)S(1)} %reshape.133, f32[2,8,128]{2,1,0:T(8,128)S(1)} %fusion.16), kind=kLoop, calls=%fused_computation.3 | loop fusion | flops 1572864 | bytes 4227072 | tf_op jit(solution)/shard_map/add | solution.py:66
  43.4 0.0 copy-start.1
  43.4 0.0 copy-start.6
  43.4 0.0 copy-start.5
  43.4 1.3 copy-done.1
  44.7 1.1 fusion.20
  45.8 0.1 fusion.10
  45.9 0.1 reshape.139
  46.0 0.1 reshape.135
  46.1 0.0 copy-done.6
  46.1 0.1 fusion.13
  46.2 14.0 %all_gather.10 = bf16[8,2,2048]{2,1,0:T(2,128)(2,1)S(1)} all-gather(bf16[1,2,2048]{2,1,0:T(2,128)(2,1)S(1)} %reshape.129), channel_id=1, replica_groups=mesh['dp'=4,'kv'=4,'tp'=2] {'kv','tp'}, dimensions={0}, use_global_device_ids=true | all-gather | bytes 73728 | tf_op jit(solution)/shard_map/all_gather | solution.py:76
  60.3 0.0 copy-done.5
  60.3 0.0 copy-start.8
  60.3 0.0 copy-start.9
  60.3 3.0 %fusion.19 = (f32[8]{0:T(128)S(1)}, f32[8]{0:T(128)S(1)}, f32[8,512]{1,0:T(8,128)S(1)}) fusion(bf16[8,2048,2]{1,0,2:T(8,128)(2,1)S(1)} %dot_general.38, bf16[2,2048,512]{2,1,0:T(8,128)(2,1)} %bitcast.56, bf16[8,512]{1,0:T(8,128)(2,1)S(1)} %copy-done.5), kind=kOutput, calls=%fused_computation.45 | convolution fusion | flops 33578992 | bytes 4284480 | tf_op jit(solution)/shard_map/atsc,tcd->asd/dot_general | solution.py:83
  63.3 2.5 %all-reduce.1 = (f32[8,1]{0,1:T(1,128)S(1)}, f32[8,1]{0,1:T(1,128)S(1)}) all-reduce(f32[8,1]{0,1:T(1,128)S(1)} %bitcast.69, f32[8,1]{0,1:T(1,128)S(1)} %bitcast.68), channel_id=1, replica_groups=mesh['dp'=4,'kv'=4,'tp'=2] {'tp'}, use_global_device_ids=true, to_apply=%region_5.6 | all-reduce | flops 16 | bytes 128 | tf_op jit(solution)/shard_map/psum | solution.py:12
  65.8 9.0 %all-reduce = (f32[8,1]{0,1:T(1,128)S(1)}, f32[8,1]{0,1:T(1,128)S(1)}) all-reduce(f32[8,1]{0,1:T(1,128)S(1)} %get-tuple-element.8, f32[8,1]{0,1:T(1,128)S(1)} %get-tuple-element.9), channel_id=1, replica_groups=mesh['dp'=4,'kv'=4,'tp'=2] {'kv'}, use_global_device_ids=true, to_apply=%region_6.7 | all-reduce | flops 16 | bytes 128 | tf_op jit(solution)/shard_map/psum | solution.py:12
  74.9 0.1 add_convert_fusion.1
  74.9 14.0 %all_gather.11 = bf16[8,4096]{1,0:T(8,128)(2,1)S(1)} all-gather(bf16[8,512]{1,0:T(8,128)(2,1)S(1)} %add_convert_fusion.1), channel_id=1, replica_groups=mesh['dp'=4,'kv'=4,'tp'=2] {'kv','tp'}, dimensions={1}, use_global_device_ids=true | all-gather | bytes 73728 | tf_op jit(solution)/shard_map/all_gather | solution.py:97
  88.9 13.5 %fusion.8 = f32[8,4096]{1,0:T(8,128)} fusion(bf16[2048,4096]{1,0:T(8,128)(2,1)} %param.29, bf16[8,4096]{1,0:T(8,128)(2,1)S(1)} %all_gather.11, bf16[4096,2048]{1,0:T(8,128)(2,1)} %param.28), kind=kOutput, calls=%fused_computation.16 | convolution fusion | flops 268484608 | bytes 33751040 | tf_op jit(solution)/shard_map/dot_general | solution.py:100
  102.4 0.0 all-reduce.4.cloned.1.call-update
  102.5 54.1 %all-reduce.4.cloned.1.call-done = f32[8,4096]{1,0:T(8,128)} async-done(((f32[8,4096]{1,0:T(8,128)}), f32[8,4096]{1,0:T(8,128)}) %all-reduce.4.cloned.1.call-update) | async-done | bytes 131088 | tf_op jit(solution)/shard_map/psum | solution.py:101
  156.5 1.1 fusion.18
  157.6 0.7 add_convert_fusion
  (26 shorter events, 0.3 us)
Async XLA Ops:
  7.2 16.1 %copy-start = (bf16[4096,8,32]{0,2,1:T(8,128)(2,1)S(1)}, bf16[4096,8,32]{0,2,1:T(8,128)(2,1)}, u32[]{:S(2)}) copy-start(bf16[4096,8,32]{0,2,1:T(8,128)(2,1)} %param.17) | copy-start | bytes 6291460
  7.2 149.3 %all-reduce.4.cloned.1.call-start = ((), (), s32[]{:S(2)}) async-start(), calls=%async_computation.1 | async-start | bytes 262144 | tf_op jit(solution)/shard_map/psum | solution.py:101
  7.2 16.7 %copy-start.4 = (bf16[4096,8,32]{0,2,1:T(8,128)(2,1)S(1)}, bf16[4096,8,32]{0,2,1:T(8,128)(2,1)}, u32[]{:S(2)}) copy-start(bf16[4096,8,32]{0,2,1:T(8,128)(2,1)} %param.18) | copy-start | bytes 6291460
  23.9 3.2 %copy-start.2 = (bf16[4096,8,64]{0,2,1:T(8,128)(2,1)S(1)}, bf16[4096,8,64]{0,2,1:T(8,128)(2,1)}, u32[]{:S(2)}) copy-start(bf16[4096,8,64]{0,2,1:T(8,128)(2,1)} %param.19) | copy-start | bytes 12582916
  27.2 2.2 %copy-start.3 = (bf16[4096,8,64]{0,2,1:T(8,128)(2,1)S(1)}, bf16[4096,8,64]{0,2,1:T(8,128)(2,1)}, u32[]{:S(2)}) copy-start(bf16[4096,8,64]{0,2,1:T(8,128)(2,1)} %param.20) | copy-start | bytes 12582916
  29.4 12.1 %copy-start.7 = (f32[8,128]{1,0:T(8,128)S(1)}, f32[8,128]{1,0:T(8,128)}, u32[]{:S(2)}) copy-start(f32[8,128]{1,0:T(8,128)} %param.22) | copy-start | bytes 12292
  43.4 1.3 copy-start.1
  43.4 2.7 %copy-start.6 = (f32[8,256]{1,0:T(8,128)S(1)}, f32[8,256]{1,0:T(8,128)}, u32[]{:S(2)}) copy-start(f32[8,256]{1,0:T(8,128)} %param.24) | copy-start | bytes 24580
  43.4 16.9 %copy-start.5 = (bf16[8,512]{1,0:T(8,128)(2,1)S(1)}, bf16[8,512]{1,0:T(8,128)(2,1)}, u32[]{:S(2)}) copy-start(bf16[8,512]{1,0:T(8,128)(2,1)} %param.16) | copy-start | bytes 24580
  60.3 14.6 %copy-start.8 = (f32[512]{0:T(512)S(1)}, f32[512]{0:T(512)}, u32[]{:S(2)}) copy-start(f32[512]{0:T(512)} %param.27) | copy-start | bytes 6148
  60.3 14.5 %copy-start.9 = (f32[512]{0:T(512)S(1)}, f32[512]{0:T(512)}, u32[]{:S(2)}) copy-start(f32[512]{0:T(512)} %param.26) | copy-start | bytes 6148
  88.9 68.7 %copy-start.10 = (f32[512]{0:T(512)S(1)}, f32[512]{0:T(512)}, u32[]{:S(2)}) copy-start(f32[512]{0:T(512)} %param.31) | copy-start | bytes 6148
  88.9 68.7 %copy-start.11 = (f32[512]{0:T(512)S(1)}, f32[512]{0:T(512)}, u32[]{:S(2)}) copy-start(f32[512]{0:T(512)} %param.30) | copy-start | bytes 6148
Sparse Core Ops, SparseCore 0:
  102.6 53.8 all-reduce.3
